TPU v7x, 32 devices: a whole 2x2x4 slice. The times are simulated.
32 devices in a mesh: sp: 8 (over z, y), tp: 4 (over x, core).
Axes of the slice: x: 2, y: 2, z: 4, core: 2. Of those that a mesh axis runs over, the one named last changes fastest.
Arguments:
- stream: bfloat16 [3072, 2048], P(('sp', 'tp')), may hold values from -6 to 6
- query_projected: bfloat16 [3072, 1024], P('sp', 'tp'), may hold values from -6 to 6
- key_projected: bfloat16 [3072, 1024], P('sp', 'tp'), may hold values from -6 to 6
- value_projected: bfloat16 [3072, 1024], P('sp', 'tp'), may hold values from -6 to 6
- gate_projected: bfloat16 [3072, 1024], P('sp', 'tp'), may hold values from -6 to 6
- strength_logits: bfloat16 [8, 3072], P('tp', 'sp'), may hold values from -7 to 4
- decay_preactivation: bfloat16 [8, 3072], P('tp', 'sp'), may hold values from -9 to 9
- extra_log_decay: float32 [8, 3072], P('tp', 'sp'), may hold values from -0.7 to 0
- head_decay_rate: float32 [8], P('tp'), may hold values from 0 to 0.1
- head_norm_gain: float32 [128], replicated, may hold values from 0.1 to 1.9
- head_output_matrix: bfloat16 [1024, 2048], P('tp'), may hold values from -0.1875 to 0.1875
- feed_norm_gain: float32 [2048], replicated, may hold values from 0.1 to 1.9
- gate_matrix: bfloat16 [2048, 5632], P('sp', 'tp'), may hold values from -0.125 to 0.125
- up_matrix: bfloat16 [2048, 5632], P('sp', 'tp'), may hold values from -0.125 to 0.125
- down_matrix: bfloat16 [5632, 2048], P('tp', 'sp'), may hold values from -0.078125 to 0.078125
Outputs:
- result: bfloat16 [3072, 2048], P(('sp', 'tp'))
All inputs are finite; a program needn't handle non-finite values.
Results may differ from a plain program's by a relative error of at most 0.015.
Values may be sent and summed in bfloat16 or wider, within the bound.
No kernel may reach another device: no remote copies, remote signals or barrier semaphores. Data moves between devices by JAX's collectives and lax.ppermute only.
A program may use at most 128 MiB of HBM per device.

v0:
```python
import jax
import jax.numpy as jnp
from jax import lax
from jax.sharding import PartitionSpec as P

HEAD = 128
BLOCK = 64
PRECISION_FULL = lax.Precision.HIGHEST
EPSILON = 1e-06


def from_behind(value, axis, by):
    size = lax.axis_size(axis)
    pairs = [(i, i + by) for i in range(size) if 0 <= i + by < size]
    return lax.ppermute(value, axis, pairs)


def unit_rows(tensor):
    return tensor * lax.rsqrt(jnp.sum(tensor * tensor, axis=-1, keepdims=True) + EPSILON)


def rms_scale(tensor):
    return tensor * lax.rsqrt(jnp.mean(tensor * tensor, axis=-1, keepdims=True) + EPSILON)


def unit_lower_inverse(strict_lower):
    size = strict_lower.shape[-1]
    row = jnp.arange(size)[:, None]
    column = jnp.arange(size)[None, :]

    def corner(half):
        same_pair = row // (2 * half) == column // (2 * half)
        return jnp.where(same_pair & (row // half != column // half), strict_lower, 0.0)

    inverse = jnp.eye(size, dtype=jnp.float32) - corner(1)
    half = 2
    while half < size:
        left = jnp.einsum("hnij,hnjk->hnik", inverse, corner(half), precision=PRECISION_FULL)
        inverse = inverse - jnp.einsum("hnij,hnjk->hnik", left, inverse, precision=PRECISION_FULL)
        half *= 2
    return inverse


def swap(value, axis, bit):
    size = lax.axis_size(axis)
    return lax.ppermute(value, axis, [(i, i ^ bit) for i in range(size)])


def relative_order(count):
    order = [0]
    bit = count // 2
    while bit:
        order = order + [place ^ bit for place in order]
        bit //= 2
    return order


def gather_relative(own):
    bit = lax.axis_size("tp") // 2
    while bit:
        own = jnp.concatenate([own, swap(own, "tp", bit)], axis=0)
        bit //= 2
    return own


def scatter_relative(left_rows, matrix):
    size = lax.axis_size("tp")
    if size == 1:
        return jnp.dot(left_rows, matrix, preferred_element_type=jnp.float32)
    half = left_rows.shape[0] // 2
    leaving = jnp.dot(left_rows[half:], matrix, preferred_element_type=jnp.float32)
    arrived = swap(leaving.astype(jnp.bfloat16), "tp", 1)
    total = jnp.dot(left_rows[:half], matrix, preferred_element_type=jnp.float32)
    total = total + arrived.astype(jnp.float32)
    bit = 2
    while bit < size:
        half = total.shape[0] // 2
        arrived = swap(total[half:].astype(jnp.bfloat16), "tp", bit)
        total = total[:half] + arrived.astype(jnp.float32)
        bit *= 2
    return total


def inflow_of_earlier(matrix_product, running_state):
    size = lax.axis_size("sp")
    width = running_state.shape[-1]
    pair = jnp.concatenate([matrix_product, running_state], axis=-1)
    pair = from_behind(pair.astype(jnp.bfloat16), "sp", 1).astype(jnp.float32)
    by = 1
    while by < size - 1:
        matrix, state = (pair[..., :width], pair[..., width:])
        last = 2 * by >= size - 1
        sent = (state if last else pair).astype(jnp.bfloat16)
        earlier = from_behind(sent, "sp", by).astype(jnp.float32)
        moved = jnp.einsum("hij,hjk->hik", matrix, earlier, precision=PRECISION_FULL)
        if last:
            pair = jnp.concatenate([matrix, state + moved], axis=-1)
        else:
            pair = jnp.concatenate([moved[..., :width], state + moved[..., width:]], axis=-1)
        by *= 2
    return pair[..., width:]


def block_correction(
    unit_queries,
    unit_keys,
    complete_values,
    strength_logits,
    decay_preactivation,
    extra_log_decay,
    head_decay_rate,
):
    head_count, length, head_width = unit_queries.shape
    block_count = length // BLOCK

    def to_blocks(tensor):
        return tensor.reshape((head_count, block_count, BLOCK) + tensor.shape[2:])

    beta_gate = jax.nn.sigmoid(strength_logits.astype(jnp.float32))
    decay_logarithm = (
        -head_decay_rate[:, None] * jax.nn.softplus(decay_preactivation.astype(jnp.float32))
        + extra_log_decay
    )
    query_block = to_blocks(unit_queries)
    key_block = to_blocks(unit_keys)
    value_block = to_blocks(complete_values)
    beta_block = to_blocks(beta_gate)
    cumulative = jnp.cumsum(to_blocks(decay_logarithm), axis=-1)
    causal = jnp.tril(jnp.ones((BLOCK, BLOCK), bool))
    strict = jnp.tril(jnp.ones((BLOCK, BLOCK), bool), -1)
    spread = cumulative[..., :, None] - cumulative[..., None, :]
    damping = jnp.where(causal, jnp.exp(jnp.where(causal, spread, 0.0)), 0.0)
    key_beta = key_block * beta_block[..., None]
    lower_part = jnp.einsum(
        "hnid,hnjd->hnij", key_beta, key_block, precision=PRECISION_FULL
    ) * jnp.where(strict, damping, 0.0)
    right_side = jnp.concatenate(
        [value_block * beta_block[..., None], key_beta * jnp.exp(cumulative)[..., None]], axis=-1
    )
    solved = jnp.einsum(
        "hnij,hnjd->hnid", unit_lower_inverse(lower_part), right_side, precision=PRECISION_FULL
    )
    target_values = solved[..., :head_width]
    householder_weights = solved[..., head_width:]
    inner_scores = (
        jnp.einsum("hnid,hnjd->hnij", query_block, key_block, precision=PRECISION_FULL) * damping
    )
    decayed_queries = query_block * jnp.exp(cumulative)[..., None]
    closing_log_decay = cumulative[..., -1:]
    decayed_keys = key_block * jnp.exp(closing_log_decay - cumulative)[..., None]
    return (
        decayed_queries,
        decayed_keys,
        target_values,
        householder_weights,
        inner_scores,
        closing_log_decay,
    )


def local_recurrence(
    query_projected,
    key_projected,
    value_projected,
    strength_logits,
    decay_preactivation,
    extra_log_decay,
    head_decay_rate,
):
    head_count = strength_logits.shape[0]
    tok_count = strength_logits.shape[1]

    def split_heads(tensor):
        return tensor.reshape(tok_count, head_count, HEAD).transpose(1, 0, 2).astype(jnp.float32)

    unit_queries = unit_rows(split_heads(query_projected)) * HEAD ** (-0.5)
    unit_keys = unit_rows(split_heads(key_projected))
    complete_values = split_heads(value_projected)
    score_terms = block_correction(
        unit_queries,
        unit_keys,
        complete_values,
        strength_logits,
        decay_preactivation,
        extra_log_decay,
        head_decay_rate,
    )
    identity = jnp.broadcast_to(jnp.eye(HEAD, dtype=jnp.float32), (head_count, HEAD, HEAD))

    def advance(carry, items):
        running_state, matrix_product = carry
        (
            decayed_queries,
            decayed_keys,
            target_values,
            householder_weights,
            inner_scores,
            closing_log_decay,
        ) = items
        new_state = target_values - jnp.einsum(
            "fdc,fcj->fdj", householder_weights, running_state, precision=PRECISION_FULL
        )
        layer_output = jnp.einsum(
            "fdc,fcj->fdj", decayed_queries, running_state, precision=PRECISION_FULL
        )
        layer_output = layer_output + jnp.einsum(
            "hij,hjv->hiv", inner_scores, new_state, precision=PRECISION_FULL
        )
        passed_state = decayed_queries - jnp.einsum(
            "hij,hjk->hik", inner_scores, householder_weights, precision=PRECISION_FULL
        )
        decay_span = jnp.einsum(
            "fdc,fcj->fdj", passed_state, matrix_product, precision=PRECISION_FULL
        )
        decay_factor = jnp.exp(closing_log_decay)[:, :, None]
        step_map = decay_factor * identity - jnp.einsum(
            "hik,hij->hkj", decayed_keys, householder_weights, precision=PRECISION_FULL
        )
        running_state = decay_factor * running_state + jnp.einsum(
            "xwp,xws->xps", decayed_keys, new_state, precision=PRECISION_FULL
        )
        matrix_product = jnp.einsum(
            "hij,hjk->hik", step_map, matrix_product, precision=PRECISION_FULL
        )
        return ((running_state, matrix_product), (layer_output, decay_span))

    moved = tuple((jnp.moveaxis(tensor, 1, 0) for tensor in score_terms))
    zeros_state = jnp.zeros((head_count, HEAD, HEAD), jnp.float32)
    (running_state, matrix_product), (block_outputs, decay_spans) = lax.scan(
        advance, (zeros_state, identity), moved
    )

    def merge_blocks(tensor):
        return jnp.moveaxis(tensor, 0, 1).reshape(head_count, tok_count, HEAD)

    return (
        merge_blocks(block_outputs),
        merge_blocks(decay_spans),
        matrix_product,
        running_state,
        identity,
    )


def body(
    stream,
    query_projected,
    key_projected,
    value_projected,
    gate_projected,
    strength_logits,
    decay_preactivation,
    extra_log_decay,
    head_decay_rate,
    head_norm_gain,
    head_output_matrix,
    feed_norm_gain,
    gate_matrix,
    up_matrix,
    down_matrix,
):
    gate_whole = lax.all_gather(gate_matrix, "sp", axis=0, tiled=True)
    up_whole = lax.all_gather(up_matrix, "sp", axis=0, tiled=True)
    down_whole = lax.all_gather(down_matrix, "sp", axis=1, tiled=True)
    block_outputs, decay_spans, matrix_product, running_state, _ = local_recurrence(
        query_projected,
        key_projected,
        value_projected,
        strength_logits,
        decay_preactivation,
        extra_log_decay,
        head_decay_rate,
    )
    state_inflow = inflow_of_earlier(matrix_product, running_state)
    attention_output = block_outputs + jnp.einsum(
        "qwc,qcn->qwn", decay_spans, state_inflow, precision=PRECISION_FULL
    )
    head_count = attention_output.shape[0]
    tok_count = attention_output.shape[1]
    normed_heads = rms_scale(attention_output) * head_norm_gain
    gated = normed_heads.transpose(1, 0, 2).reshape(tok_count, head_count * HEAD)
    mixed = (gated * jax.nn.silu(gate_projected.astype(jnp.float32))).astype(jnp.bfloat16)
    tp_size = lax.axis_size("tp")
    tp_index = lax.axis_index("tp")
    chunks = mixed.reshape(tp_size, tok_count // tp_size, head_count * HEAD)
    ordered = jnp.concatenate(
        [
            lax.dynamic_index_in_dim(chunks, tp_index ^ place, 0, keepdims=False)
            for place in relative_order(tp_size)
        ],
        axis=0,
    )
    branch = scatter_relative(ordered, head_output_matrix)
    residual_own = stream.astype(jnp.float32) + branch
    normed_own = (rms_scale(residual_own) * feed_norm_gain).astype(jnp.bfloat16)
    whole_rows = gather_relative(normed_own)
    gate_total = jnp.dot(whole_rows, gate_whole, preferred_element_type=jnp.float32)
    up_total = jnp.dot(whole_rows, up_whole, preferred_element_type=jnp.float32)
    hidden = (jax.nn.silu(gate_total) * up_total).astype(jnp.bfloat16)
    ffn_own = scatter_relative(hidden, down_whole)
    return (residual_own + ffn_own).astype(jnp.bfloat16)


def solution(mesh):
    placed = (
        P(("sp", "tp"), None),
        P("sp", "tp"),
        P("sp", "tp"),
        P("sp", "tp"),
        P("sp", "tp"),
        P("tp", "sp"),
        P("tp", "sp"),
        P("tp", "sp"),
        P("tp"),
        P(),
        P("tp", None),
        P(),
        P("sp", "tp"),
        P("sp", "tp"),
        P("tp", "sp"),
    )
    return jax.shard_map(
        body, mesh=mesh, in_specs=placed, out_specs=P(("sp", "tp"), None), check_vma=False
    )
```

profile of v0, /device:TPU:0, one launch (start us, length us, event | category | flops | bytes accessed | tf_op | source)
XLA Modules:
  0.0 326.3 jit_solution(2462705551969413879)
XLA Ops:
  6.6 0.7 all-gather.4.cloned.1.call-update
  7.3 0.7 all-gather.6.cloned.1.call-update
  8.1 0.7 all-gather.8.cloned.1.call-update
  10.2 0.8 convolution_multiply_fusion
  17.4 0.8 fusion.42
  18.3 0.8 slice_bitcast_fusion
  19.1 0.8 fusion.38
  20.0 26.2 %while.17 = (s32[]{:T(128)}, f32[2,128,128]{2,1,0:T(8,128)S(1)}, f32[2,128,128]{2,1,0:T(8,128)S(1)}, f32[6,2,64,128]{3,2,0,1:T(8,128)}, f32[6,2,64,128]{3,2,0,1:...) while((s32[]{:T(128)}, f32[2,128,128]{2,1,0:T(8,128)S(1)}, ...), condition=%wide.region_4.5_spmd.clone, body=%wide.region_3.4_spmd.clone.sunk | while | flops 201605120 | bytes 2758829 | solution.py:229
  20.0 1.1 convolution_subtract_fusion.11
  21.4 0.8 fusion.205
  22.8 0.9 fusion.206
  24.4 1.1 convolution_subtract_fusion.11
  25.7 0.8 fusion.205
  27.2 0.9 fusion.206
  28.7 1.1 convolution_subtract_fusion.11
  30.1 0.8 fusion.205
  31.6 0.9 fusion.206
  33.1 1.1 convolution_subtract_fusion.11
  34.5 0.8 fusion.205
  35.9 0.9 fusion.206
  37.5 1.1 convolution_subtract_fusion.11
  38.8 0.8 fusion.205
  40.3 0.9 fusion.206
  41.8 1.1 convolution_subtract_fusion.11
  43.2 0.8 fusion.205
  44.7 0.9 fusion.206
  46.3 5.0 %collective-permute-start = (bf16[2,128,256]{2,1,0:T(8,128)(2,1)S(1)}, bf16[2,128,256]{2,1,0:T(8,128)(2,1)S(1)}, u32[]{:S(2)}, u32[]{:S(2)}) collective-permute-start(bf16[2,128,256]{2,1,0:T(8,128)(2,1)S(1)} %pad_maximum_fusion.6), channel_id=1, source_target_pairs={{0,4},{4,8},{8,12},{12,16},{16,20},{20,24},{24,28},{1,5},{5,9},{9,... | collective-permute-start | bytes 393224 | tf_op jit(solution)/shard_map/ppermute | solution.py:15
  51.3 5.5 %collective-permute-done = bf16[2,128,256]{2,1,0:T(8,128)(2,1)S(1)} collective-permute-done((bf16[2,128,256]{2,1,0:T(8,128)(2,1)S(1)}, bf16[2,128,256]{2,1,0:T(8,128)(2,1)S(1)}, u32[]{:S(2)}, u32[]{:S(2)}) %collective-permute-start) | collective-permute-done | bytes 131104 | tf_op jit(solution)/shard_map/ppermute | solution.py:15
  56.9 4.4 %collective-permute-start.1 = (bf16[2,128,256]{2,1,0:T(8,128)(2,1)S(1)}, bf16[2,128,256]{2,1,0:T(8,128)(2,1)S(1)}, u32[]{:S(2)}, u32[]{:S(2)}) collective-permute-start(bf16[2,128,256]{2,1,0:T(8,128)(2,1)S(1)} %collective-permute-done), channel_id=1, source_target_pairs={{0,4},{4,8},{8,12},{12,16},{16,20},{20,24},{24,28},{1,5},{5,9},{9,... | collective-permute-start | bytes 393224 | tf_op jit(solution)/shard_map/ppermute | solution.py:15
  61.2 5.4 %collective-permute-done.1 = bf16[2,128,256]{2,1,0:T(8,128)(2,1)S(1)} collective-permute-done((bf16[2,128,256]{2,1,0:T(8,128)(2,1)S(1)}, bf16[2,128,256]{2,1,0:T(8,128)(2,1)S(1)}, u32[]{:S(2)}, u32[]{:S(2)}) %collective-permute-start.1) | collective-permute-done | bytes 131104 | tf_op jit(solution)/shard_map/ppermute | solution.py:15
  66.9 6.0 %collective-permute-start.2 = (bf16[2,128,256]{2,1,0:T(8,128)(2,1)S(1)}, bf16[2,128,256]{2,1,0:T(8,128)(2,1)S(1)}, u32[]{:S(2)}, u32[]{:S(2)}) collective-permute-start(bf16[2,128,256]{2,1,0:T(8,128)(2,1)S(1)} %pad_maximum_fusion.7), channel_id=1, source_target_pairs={{0,8},{4,12},{8,16},{12,20},{16,24},{20,28},{1,9},{5,13},{9,17},{1... | collective-permute-start | bytes 393224 | tf_op jit(solution)/shard_map/ppermute | solution.py:15
  72.9 5.4 %collective-permute-done.2 = bf16[2,128,256]{2,1,0:T(8,128)(2,1)S(1)} collective-permute-done((bf16[2,128,256]{2,1,0:T(8,128)(2,1)S(1)}, bf16[2,128,256]{2,1,0:T(8,128)(2,1)S(1)}, u32[]{:S(2)}, u32[]{:S(2)}) %collective-permute-start.2) | collective-permute-done | bytes 131104 | tf_op jit(solution)/shard_map/ppermute | solution.py:15
  78.6 20.5 %collective-permute-start.3 = (bf16[2,128,128]{2,1,0:T(8,128)(2,1)S(1)}, bf16[2,128,128]{2,1,0:T(8,128)(2,1)S(1)}, u32[]{:S(2)}, u32[]{:S(2)}) collective-permute-start(bf16[2,128,128]{2,1,0:T(8,128)(2,1)S(1)} %fusion.128), channel_id=1, source_target_pairs={{0,16},{4,20},{8,24},{12,28},{1,17},{5,21},{9,25},{13,29},{2,18},{... | collective-permute-start | bytes 196616 | tf_op jit(solution)/shard_map/ppermute | solution.py:15
  99.3 2.9 collective-permute-done.3
  104.1 2.3 collective-permute-done.4
  106.9 11.1 %collective-permute-done.5 = bf16[96,2048]{1,0:T(8,128)(2,1)S(1)} collective-permute-done((bf16[96,2048]{1,0:T(8,128)(2,1)S(1)}, bf16[96,2048]{1,0:T(8,128)(2,1)S(1)}, u32[]{:S(2)}, u32[]{:S(2)}) %collective-permute-start.5) | collective-permute-done | bytes 393248 | tf_op jit(solution)/shard_map/ppermute | solution.py:46
  118.8 10.0 %collective-permute-done.6 = bf16[96,2048]{1,0:T(8,128)(2,1)S(1)} collective-permute-done((bf16[96,2048]{1,0:T(8,128)(2,1)S(1)}, bf16[96,2048]{1,0:T(8,128)(2,1)S(1)}, u32[]{:S(2)}, u32[]{:S(2)}) %collective-permute-start.6) | collective-permute-done | bytes 393248 | tf_op jit(solution)/shard_map/ppermute | solution.py:46
  129.6 1.8 collective-permute-done.7
  131.4 7.1 %fusion.47 = f32[384,1408]{1,0:T(8,128)} fusion(bf16[2048,1408]{1,0:T(8,128)(2,1)} %all-gather.4.cloned.1.call-done, bf16[192,2048]{1,0:T(8,128)(2,1)} %collective-permute-done.7, bf16[96,2048]{1,0:T(8,128)(2,1)} %copy-done.7, bf16[96,2048]{1,0:T(8,128)(2,1)} %copy-done.2), kind=kOutput, calls=%fused_computation.75 | convolution fusion | flops 2219311104 | bytes 9502720 | tf_op jit(solution)/shard_map/dot_general | solution.py:297
  138.5 67.4 %all-gather.6.cloned.1.call-done = bf16[2048,1408]{1,0:T(8,128)(2,1)} async-done(((bf16[256,1408]{1,0:T(8,128)(2,1)}), bf16[2048,1408]{1,0:T(8,128)(2,1)}) %all-gather.6.cloned.1.call-update) | async-done | bytes 5767184 | tf_op jit(solution)/shard_map/all_gather | solution.py:263
  206.0 7.4 %multiply_convert_fusion = bf16[384,1408]{1,0:T(8,128)(2,1)} fusion(f32[384,1408]{1,0:T(8,128)} %fusion.47, bf16[2048,1408]{1,0:T(8,128)(2,1)} %all-gather.6.cloned.1.call-done, bf16[192,2048]{1,0:T(8,128)(2,1)} %collective-permute-done.7, bf16[96,2048]{1,0:T(8,128)(2,1)} %copy-done.7, bf16[96,2048]{1,0:T(8,128)(2,1)} %copy-done.2), kind=kOutput, calls=%fused_computation.46 | convolution fusion | flops 2222555136 | bytes 10584064 | tf_op jit(solution)/shard_map/dot_general | solution.py:298
  213.4 86.0 %all-gather.8.cloned.1.call-done = bf16[1408,2048]{1,0:T(8,128)(2,1)} async-done(((bf16[1408,256]{1,0:T(8,128)(2,1)}), bf16[1408,2048]{1,0:T(8,128)(2,1)}) %all-gather.8.cloned.1.call-update) | async-done | bytes 5767184 | tf_op jit(solution)/shard_map/all_gather | solution.py:264
  299.4 4.3 %convolution_convert_fusion = bf16[192,2048]{1,0:T(8,128)(2,1)S(1)} fusion(bf16[1408,2048]{1,0:T(8,128)(2,1)} %all-gather.8.cloned.1.call-done, bf16[384,1408]{1,0:T(8,128)(2,1)} %multiply_convert_fusion), kind=kOutput, calls=%fused_computation.44 | convolution fusion | flops 1107689472 | bytes 7094272 | tf_op jit(solution)/shard_map/dot_general | solution.py:71
  303.8 2.3 collective-permute-done.8
  306.1 1.4 convert_add_fusion
  307.5 1.6 collective-permute-start.9
  309.1 9.6 %collective-permute-done.9 = bf16[96,2048]{1,0:T(8,128)(2,1)S(1)} collective-permute-done((bf16[96,2048]{1,0:T(8,128)(2,1)S(1)}, bf16[96,2048]{1,0:T(8,128)(2,1)S(1)}, u32[]{:S(2)}, u32[]{:S(2)}) %collective-permute-start.9) | collective-permute-done | bytes 393248 | tf_op jit(solution)/shard_map/ppermute | solution.py:46
  318.7 1.0 fusion.40
  (151 shorter events, 21.5 us)
Async XLA Ops:
  6.5 97.1 %copy-start = (bf16[256,2048]{1,0:T(8,128)(2,1)S(1)}, bf16[256,2048]{1,0:T(8,128)(2,1)}, u32[]{:S(2)}) copy-start(bf16[256,2048]{1,0:T(8,128)(2,1)} %param.27) | copy-start | bytes 3145732
  6.5 2.3 copy-start.16
  6.5 2.4 copy-start.12
  6.5 2.4 copy-start.11
  6.5 2.5 copy-start.3
  6.5 3.0 copy-start.13
  6.6 124.9 %all-gather.4.cloned.1.call-start = ((), (), s32[]{:S(2)}) async-start(), calls=%async_computation | async-start | bytes 6488064 | tf_op jit(solution)/shard_map/all_gather | solution.py:262
  7.3 198.7 %all-gather.6.cloned.1.call-start = ((), (), s32[]{:S(2)}) async-start(), calls=%async_computation.1 | async-start | bytes 6488064 | tf_op jit(solution)/shard_map/all_gather | solution.py:263
  8.0 291.3 %all-gather.8.cloned.1.call-start = ((), (), s32[]{:S(2)}) async-start(), calls=%async_computation.2 | async-start | bytes 6488064 | tf_op jit(solution)/shard_map/all_gather | solution.py:264
  14.4 2.3 copy-start.4
  14.9 2.1 copy-start.8
  46.2 52.9 %copy-start.5 = (f32[6,2,64,128]{3,2,0,1:T(8,128)S(1)}, f32[6,2,64,128]{3,2,0,1:T(8,128)}, u32[]{:S(2)}) copy-start(f32[6,2,64,128]{3,2,0,1:T(8,128)} %get-tuple-element.70) | copy-start | bytes 1179652
  46.2 56.2 %copy-start.6 = (f32[6,2,64,128]{3,2,0,1:T(8,128)S(1)}, f32[6,2,64,128]{3,2,0,1:T(8,128)}, u32[]{:S(2)}) copy-start(f32[6,2,64,128]{3,2,0,1:T(8,128)} %get-tuple-element.71) | copy-start | bytes 1179652
  46.3 10.6 %collective-permute-start = (bf16[2,128,256]{2,1,0:T(8,128)(2,1)S(1)}, bf16[2,128,256]{2,1,0:T(8,128)(2,1)S(1)}, u32[]{:S(2)}, u32[]{:S(2)}) collective-permute-start(bf16[2,128,256]{2,1,0:T(8,128)(2,1)S(1)} %pad_maximum_fusion.6), channel_id=1, source_target_pairs={{0,4},{4,8},{8,12},{12,16},{16,20},{20,24},{24,28},{1,5},{5,9},{9,... | collective-permute-start | bytes 393224 | tf_op jit(solution)/shard_map/ppermute | solution.py:15
  56.9 9.8 %collective-permute-start.1 = (bf16[2,128,256]{2,1,0:T(8,128)(2,1)S(1)}, bf16[2,128,256]{2,1,0:T(8,128)(2,1)S(1)}, u32[]{:S(2)}, u32[]{:S(2)}) collective-permute-start(bf16[2,128,256]{2,1,0:T(8,128)(2,1)S(1)} %collective-permute-done), channel_id=1, source_target_pairs={{0,4},{4,8},{8,12},{12,16},{16,20},{20,24},{24,28},{1,5},{5,9},{9,... | collective-permute-start | bytes 393224 | tf_op jit(solution)/shard_map/ppermute | solution.py:15
  66.8 36.3 %copy-start.14 = (f32[128]{0:T(128)S(1)}, f32[128]{0:T(128)}, u32[]{:S(2)}) copy-start(f32[128]{0:T(128)} %param.26) | copy-start | bytes 1540
  66.9 11.4 %collective-permute-start.2 = (bf16[2,128,256]{2,1,0:T(8,128)(2,1)S(1)}, bf16[2,128,256]{2,1,0:T(8,128)(2,1)S(1)}, u32[]{:S(2)}, u32[]{:S(2)}) collective-permute-start(bf16[2,128,256]{2,1,0:T(8,128)(2,1)S(1)} %pad_maximum_fusion.7), channel_id=1, source_target_pairs={{0,8},{4,12},{8,16},{12,20},{16,24},{20,28},{1,9},{5,13},{9,17},{1... | collective-permute-start | bytes 393224 | tf_op jit(solution)/shard_map/ppermute | solution.py:15
  78.6 24.8 %copy-start.9 = (bf16[384,256]{1,0:T(8,128)(2,1)S(1)}, bf16[384,256]{1,0:T(8,128)(2,1)}, u32[]{:S(2)}) copy-start(bf16[384,256]{1,0:T(8,128)(2,1)} %param.21) | copy-start | bytes 589828
  78.6 23.6 %collective-permute-start.3 = (bf16[2,128,128]{2,1,0:T(8,128)(2,1)S(1)}, bf16[2,128,128]{2,1,0:T(8,128)(2,1)S(1)}, u32[]{:S(2)}, u32[]{:S(2)}) collective-permute-start(bf16[2,128,128]{2,1,0:T(8,128)(2,1)S(1)} %fusion.128), channel_id=1, source_target_pairs={{0,16},{4,20},{8,24},{12,28},{1,17},{5,21},{9,25},{13,29},{2,18},{... | collective-permute-start | bytes 196616 | tf_op jit(solution)/shard_map/ppermute | solution.py:15
  104.0 14.0 %copy-start.1 = (bf16[96,2048]{1,0:T(8,128)(2,1)S(1)}, bf16[96,2048]{1,0:T(8,128)(2,1)}, u32[]{:S(2)}) copy-start(bf16[96,2048]{1,0:T(8,128)(2,1)} %param.17) | copy-start | bytes 1179652
  104.0 2.4 collective-permute-start.4
  106.3 11.9 %copy-start.10 = (f32[2048]{0:T(1024)S(1)}, f32[2048]{0:T(1024)}, u32[]{:S(2)}) copy-start(f32[2048]{0:T(1024)} %param.28) | copy-start | bytes 24580
  106.8 11.2 %collective-permute-start.5 = (bf16[96,2048]{1,0:T(8,128)(2,1)S(1)}, bf16[96,2048]{1,0:T(8,128)(2,1)S(1)}, u32[]{:S(2)}, u32[]{:S(2)}) collective-permute-start(bf16[96,2048]{1,0:T(8,128)(2,1)S(1)} %slice.148), channel_id=1, source_target_pairs={{0,2},{1,3},{2,0},{3,1},{4,6},{5,7},{6,4},{7,5},{8,10},{9,11},{10,... | collective-permute-start | bytes 1179656 | tf_op jit(solution)/shard_map/ppermute | solution.py:46
  118.5 10.4 %copy-start.2 = (bf16[96,2048]{1,0:T(8,128)(2,1)}, bf16[96,2048]{1,0:T(8,128)(2,1)S(1)}, u32[]{:S(2)}) copy-start(bf16[96,2048]{1,0:T(8,128)(2,1)S(1)} %multiply_convert_fusion.1) | copy-start | bytes 1179652
  118.5 10.4 %collective-permute-start.6 = (bf16[96,2048]{1,0:T(8,128)(2,1)S(1)}, bf16[96,2048]{1,0:T(8,128)(2,1)S(1)}, u32[]{:S(2)}, u32[]{:S(2)}) collective-permute-start(bf16[96,2048]{1,0:T(8,128)(2,1)S(1)} %multiply_convert_fusion.1), channel_id=1, source_target_pairs={{0,2},{1,3},{2,0},{3,1},{4,6},{5,7},{6,4},{7,5},{8,10},{9,11},{10,... | collective-permute-start | bytes 1179656 | tf_op jit(solution)/shard_map/ppermute | solution.py:46
  128.9 0.7 copy-start.7
  128.9 2.5 collective-permute-start.7
  299.4 6.7 %copy-start.15 = (bf16[1408,2048]{1,0:T(8,128)(2,1)S(1)}, bf16[1408,2048]{1,0:T(8,128)(2,1)}, u32[]{:S(2)}) copy-start(bf16[1408,2048]{1,0:T(8,128)(2,1)} %all-gather.8.cloned.1.call-done) | copy-start | bytes 17301508
  299.4 6.7 %copy-start.17 = (bf16[384,1408]{1,0:T(8,128)(2,1)S(1)}, bf16[384,1408]{1,0:T(8,128)(2,1)}, u32[]{:S(2)}) copy-start(bf16[384,1408]{1,0:T(8,128)(2,1)} %multiply_convert_fusion) | copy-start | bytes 3244036
  303.7 2.4 collective-permute-start.8
  307.5 11.2 %collective-permute-start.9 = (bf16[96,2048]{1,0:T(8,128)(2,1)S(1)}, bf16[96,2048]{1,0:T(8,128)(2,1)S(1)}, u32[]{:S(2)}, u32[]{:S(2)}) collective-permute-start(bf16[96,2048]{1,0:T(8,128)(2,1)S(1)} %slice.147), channel_id=1, source_target_pairs={{0,2},{1,3},{2,0},{3,1},{4,6},{5,7},{6,4},{7,5},{8,10},{9,11},{10,... | collective-permute-start | bytes 1179656 | tf_op jit(solution)/shard_map/ppermute | solution.py:46
Sparse Core Ops, SparseCore 0:
  9.5 99.7 all-gather.3
  111.5 94.4 all-gather.5
  208.0 91.2 all-gather.7
where the time goes:
time: 327 us; the launch traced here: 326 us
  waiting for transfers between devices  212 us (65%)
  matrix products  55.6 us (17%)
  starting transfers between devices  38.3 us (12%)
  between operations  13.8 us (4%)
  other arithmetic  3.82 us (1%)
    all_gather x1, waiting for transfers between devices, body(): down_whole = lax.all_gather(down_matrix, 'sp', axis=1, tiled=True)  86 us
    all_gather x1, waiting for transfers between devices, body(): up_whole = lax.all_gather(up_matrix, 'sp', axis=0, tiled=True)  67.4 us
    ppermute x6, waiting for transfers between devices, swap(): return lax.ppermute(value, axis, [(i, i ^ bit) for i in range(size)])  37.2 us
    ppermute x4, starting transfers between devices, from_behind(): return lax.ppermute(value, axis, pairs)  35.9 us
    ppermute x4, waiting for transfers between devices, from_behind(): return lax.ppermute(value, axis, pairs)  19.2 us
    dot_general x1, matrix products, body(): up_total = jnp.dot(whole_rows, up_whole, preferred_element_type=jnp.float32)  7.38 us
    dot_general x1, matrix products, body(): jnp.dot(whole_rows, gate_whole, preferred_element_type=jnp.float32)  7.12 us
  transfers between devices with their start and end apart: 13, of which 12 were waited for; matrix products, arithmetic and copies ran while one was open for 17% of the time, Pallas kernels for 0%

commit v1 on v0

--- a/solution.py
+++ b/solution.py
@@ -260,7 +260,12 @@
     down_matrix,
 ):
     gate_whole = lax.all_gather(gate_matrix, "sp", axis=0, tiled=True)
-    up_whole = lax.all_gather(up_matrix, "sp", axis=0, tiled=True)
+    ring = [up_matrix]
+    for hop in range(7):
+        ring.append(lax.ppermute(ring[-1], "sp", [(dev, (dev + 1) % 8) for dev in range(8)]))
+    up_whole = jnp.roll(
+        jnp.concatenate(ring[::-1], axis=0), (lax.axis_index("sp") + 1) * ring[0].shape[0], axis=0
+    )
     down_whole = lax.all_gather(down_matrix, "sp", axis=1, tiled=True)
     block_outputs, decay_spans, matrix_product, running_state, _ = local_recurrence(
         query_projected,

time: 327 us -> 358 us (1.095)
  matrix products: 55.6 us -> 80.4 us
  waiting for transfers between devices: 212 us -> 191 us
  local copies, waits for them, and re-layouts: 2.49 us -> 18.6 us
  other arithmetic: 3.82 us -> 12.7 us
    ppermute x0 -> x7, waiting for transfers between devices: none -> 163 us  [body(): lax.ppermute(ring[-1], 'sp', [(dev, (dev + 1) % 8) for dev in range(8)])]
    all_gather x1, waiting for transfers between devices: 86 us -> 0.01 us  [body(): down_whole = lax.all_gather(down_matrix, 'sp', axis=1, tiled=True)]
    all_gather x1 -> x0, waiting for transfers between devices: 67.4 us -> none  [body(): up_whole = lax.all_gather(up_matrix, 'sp', axis=0, tiled=True)]
    ppermute x6, waiting for transfers between devices: 37.2 us -> 19.2 us  [swap(): return lax.ppermute(value, axis, [(i, i ^ bit) for i in range(size)])]
    unnamed x37 -> x60, local copies, waits for them, and re-layouts: 0.79 us -> 14.7 us
    ppermute x4, waiting for transfers between devices: 19.2 us -> 8.39 us  [from_behind(): return lax.ppermute(value, axis, pairs)]
    ppermute x4, starting transfers between devices: 35.9 us -> 25.3 us  [from_behind(): return lax.ppermute(value, axis, pairs)]
    ppermute x0 -> x7, starting transfers between devices: none -> 6.88 us  [body(): lax.ppermute(ring[-1], 'sp', [(dev, (dev + 1) % 8) for dev in range(8)])]
  transfers between devices with their start and end apart: 13 -> 19, of which waited for: 12 -> 14; matrix products, arithmetic and copies ran while one was open for 17% -> 28% of each run, Pallas kernels for 0% -> 0%
where the time goes in v1:
time: 358 us; the launch traced here: 355 us
  waiting for transfers between devices  191 us (53%)
  matrix products  80.4 us (22%)
  starting transfers between devices  37.8 us (11%)
  local copies, waits for them, and re-layouts  18.6 us (5%)
  between operations  14.1 us (4%)
  other arithmetic  12.7 us (4%)
    ppermute x7, waiting for transfers between devices, body(): lax.ppermute(ring[-1], 'sp', [(dev, (dev + 1) % 8) for dev in range(8)])  163 us
    ppermute x4, starting transfers between devices, from_behind(): return lax.ppermute(value, axis, pairs)  25.3 us
    ppermute x6, waiting for transfers between devices, swap(): return lax.ppermute(value, axis, [(i, i ^ bit) for i in range(size)])  19.2 us
    unnamed x60, local copies, waits for them, and re-layouts  14.7 us
    dot_general x6, matrix products, advance(): jnp.einsum('hij,hjv->hiv', inner_scores, new_state, precision=PRECISION_F...  10.1 us
    ppermute x4, waiting for transfers between devices, from_behind(): return lax.ppermute(value, axis, pairs)  8.39 us
    dot_general x6, matrix products, advance(): jnp.einsum('xwp,xws->xps', decayed_keys, new_state, precision=PRECISION_F...  7.42 us
    dot_general x6, matrix products, advance(): jnp.einsum('hik,hij->hkj', decayed_keys, householder_weights, precision=P...  7.36 us
  transfers between devices with their start and end apart: 19, of which 14 were waited for; matrix products, arithmetic and copies ran while one was open for 28% of the time, Pallas kernels for 0%

profile of v1, /device:TPU:0, one launch (start us, length us, event | category | flops | bytes accessed | tf_op | source)
XLA Modules:
  0.0 355.4 jit_solution(16551163248404086554)
XLA Ops:
  19.4 1.3 multiply_multiply_fusion
  22.4 1.5 fusion.40
  24.0 51.8 %while.17 = (s32[]{:T(128)}, f32[2,128,128]{2,1,0:T(8,128)S(1)}, f32[2,128,128]{2,1,0:T(8,128)S(1)}, f32[6,2,64,128]{3,2,0,1:T(8,128)}, f32[6,2,64,128]{3,2,0,1:...) while((s32[]{:T(128)}, f32[2,128,128]{2,1,0:T(8,128)S(1)}, ...), condition=%wide.region_4.5_spmd.clone, body=%wide.region_3.4_spmd.clone.sunk | while | flops 201605120 | bytes 2759341 | solution.py:229
  26.3 1.7 fusion.208
  27.9 1.2 convolution_add_fusion.5
  31.2 1.2 convolution_subtract_fusion.12
  34.9 1.7 fusion.208
  36.6 1.2 convolution_add_fusion.5
  39.8 1.2 convolution_subtract_fusion.12
  43.5 1.7 fusion.208
  45.2 1.2 convolution_add_fusion.5
  48.4 1.2 convolution_subtract_fusion.12
  52.1 1.7 fusion.208
  53.8 1.2 convolution_add_fusion.5
  60.7 1.7 fusion.208
  62.4 1.2 convolution_add_fusion.5
  65.6 1.2 convolution_subtract_fusion.12
  69.4 1.7 fusion.208
  71.0 1.2 convolution_add_fusion.5
  74.3 1.2 convolution_subtract_fusion.12
  75.9 4.9 %collective-permute-start = (bf16[2,128,256]{2,1,0:T(8,128)(2,1)S(1)}, bf16[2,128,256]{2,1,0:T(8,128)(2,1)S(1)}, u32[]{:S(2)}, u32[]{:S(2)}) collective-permute-start(bf16[2,128,256]{2,1,0:T(8,128)(2,1)S(1)} %pad_maximum_fusion.6), channel_id=1, source_target_pairs={{0,4},{4,8},{8,12},{12,16},{16,20},{20,24},{24,28},{1,5},{5,9},{9,... | collective-permute-start | bytes 393224 | tf_op jit(solution)/shard_map/ppermute | solution.py:15
  80.8 5.3 %collective-permute-done = bf16[2,128,256]{2,1,0:T(8,128)(2,1)S(1)} collective-permute-done((bf16[2,128,256]{2,1,0:T(8,128)(2,1)S(1)}, bf16[2,128,256]{2,1,0:T(8,128)(2,1)S(1)}, u32[]{:S(2)}, u32[]{:S(2)}) %collective-permute-start) | collective-permute-done | bytes 131104 | tf_op jit(solution)/shard_map/ppermute | solution.py:15
  86.1 4.4 %collective-permute-start.1 = (bf16[2,128,256]{2,1,0:T(8,128)(2,1)S(1)}, bf16[2,128,256]{2,1,0:T(8,128)(2,1)S(1)}, u32[]{:S(2)}, u32[]{:S(2)}) collective-permute-start(bf16[2,128,256]{2,1,0:T(8,128)(2,1)S(1)} %collective-permute-done), channel_id=1, source_target_pairs={{0,4},{4,8},{8,12},{12,16},{16,20},{20,24},{24,28},{1,5},{5,9},{9,... | collective-permute-start | bytes 393224 | tf_op jit(solution)/shard_map/ppermute | solution.py:15
  90.5 2.9 collective-permute-start.8
  93.9 10.1 %collective-permute-start.2 = (bf16[2,128,256]{2,1,0:T(8,128)(2,1)S(1)}, bf16[2,128,256]{2,1,0:T(8,128)(2,1)S(1)}, u32[]{:S(2)}, u32[]{:S(2)}) collective-permute-start(bf16[2,128,256]{2,1,0:T(8,128)(2,1)S(1)} %pad_maximum_fusion.7), channel_id=1, source_target_pairs={{0,8},{4,12},{8,16},{12,20},{16,24},{20,28},{1,9},{5,13},{9,17},{1... | collective-permute-start | bytes 393224 | tf_op jit(solution)/shard_map/ppermute | solution.py:15
  104.0 2.5 collective-permute-done.2
  106.8 15.4 %collective-permute-done.8 = bf16[256,1408]{1,0:T(8,128)(2,1)S(1)} collective-permute-done((bf16[256,1408]{1,0:T(8,128)(2,1)S(1)}, bf16[256,1408]{1,0:T(8,128)(2,1)S(1)}, u32[]{:S(2)}, u32[]{:S(2)}) %collective-permute-start.8) | collective-permute-done | bytes 720928 | tf_op jit(solution)/shard_map/ppermute | solution.py:265
  122.3 2.9 collective-permute-start.9
  125.8 5.9 %collective-permute-start.3 = (bf16[2,128,128]{2,1,0:T(8,128)(2,1)}, bf16[2,128,128]{2,1,0:T(8,128)(2,1)}, u32[]{:S(2)}, u32[]{:S(2)}) collective-permute-start(bf16[2,128,128]{2,1,0:T(8,128)(2,1)} %fusion.132), channel_id=1, source_target_pairs={{0,16},{4,20},{8,24},{12,28},{1,17},{5,21},{9,25},{13,29},{2,18},{... | collective-permute-start | bytes 196616 | tf_op jit(solution)/shard_map/ppermute | solution.py:15
  134.5 1.7 multiply_reduce_fusion.1
  136.2 10.9 %collective-permute-done.9 = bf16[256,1408]{1,0:T(8,128)(2,1)S(1)} collective-permute-done((bf16[256,1408]{1,0:T(8,128)(2,1)S(1)}, bf16[256,1408]{1,0:T(8,128)(2,1)S(1)}, u32[]{:S(2)}, u32[]{:S(2)}) %collective-permute-start.9) | collective-permute-done | bytes 720928 | tf_op jit(solution)/shard_map/ppermute | solution.py:265
  151.3 35.6 %collective-permute-done.10 = bf16[256,1408]{1,0:T(8,128)(2,1)} collective-permute-done((bf16[256,1408]{1,0:T(8,128)(2,1)S(1)}, bf16[256,1408]{1,0:T(8,128)(2,1)}, u32[]{:S(2)}, u32[]{:S(2)}) %collective-permute-start.10) | collective-permute-done | bytes 720928 | tf_op jit(solution)/shard_map/ppermute | solution.py:265
  187.3 34.9 %collective-permute-done.11 = bf16[256,1408]{1,0:T(8,128)(2,1)S(1)} collective-permute-done((bf16[256,1408]{1,0:T(8,128)(2,1)}, bf16[256,1408]{1,0:T(8,128)(2,1)S(1)}, u32[]{:S(2)}, u32[]{:S(2)}) %collective-permute-start.11) | collective-permute-done | bytes 720928 | tf_op jit(solution)/shard_map/ppermute | solution.py:265
  222.7 1.8 collective-permute-start.5
  224.5 33.1 %collective-permute-done.12 = bf16[256,1408]{1,0:T(8,128)(2,1)S(1)} collective-permute-done((bf16[256,1408]{1,0:T(8,128)(2,1)S(1)}, bf16[256,1408]{1,0:T(8,128)(2,1)S(1)}, u32[]{:S(2)}, u32[]{:S(2)}) %collective-permute-start.12) | collective-permute-done | bytes 720928 | tf_op jit(solution)/shard_map/ppermute | solution.py:265
  258.5 25.7 %collective-permute-done.13 = bf16[256,1408]{1,0:T(8,128)(2,1)} collective-permute-done((bf16[256,1408]{1,0:T(8,128)(2,1)S(1)}, bf16[256,1408]{1,0:T(8,128)(2,1)}, u32[]{:S(2)}, u32[]{:S(2)}) %collective-permute-start.13) | collective-permute-done | bytes 720928 | tf_op jit(solution)/shard_map/ppermute | solution.py:265
  285.1 1.7 collective-permute-start.6
  286.8 7.5 %collective-permute-done.6 = bf16[96,2048]{1,0:T(8,128)(2,1)} collective-permute-done((bf16[96,2048]{1,0:T(8,128)(2,1)}, bf16[96,2048]{1,0:T(8,128)(2,1)}, u32[]{:S(2)}, u32[]{:S(2)}) %collective-permute-start.6) | collective-permute-done | bytes 393248 | tf_op jit(solution)/shard_map/ppermute | solution.py:46
  295.5 7.4 %collective-permute-done.14 = bf16[256,1408]{1,0:T(8,128)(2,1)} collective-permute-done((bf16[256,1408]{1,0:T(8,128)(2,1)}, bf16[256,1408]{1,0:T(8,128)(2,1)}, u32[]{:S(2)}, u32[]{:S(2)}) %collective-permute-start.14) | collective-permute-done | bytes 720928 | tf_op jit(solution)/shard_map/ppermute | solution.py:265
  305.3 1.3 constant_dynamic-update-slice_fusion.13
  312.3 4.3 %copy-done.16 = bf16[4096,1408]{1,0:T(8,128)(2,1)} copy-done((bf16[4096,1408]{1,0:T(8,128)(2,1)}, bf16[4096,1408]{1,0:T(8,128)(2,1)S(1)}, u32[]{:S(2)}) %copy-start.16) | copy-done | bytes 11534360
  316.5 5.8 %fusion.48 = f32[384,1408]{1,0:T(8,128)S(1)} fusion(bf16[2048,1408]{1,0:T(8,128)(2,1)} %all-gather.3.cloned.1.call-done, bf16[192,2048]{1,0:T(8,128)(2,1)} %collective-permute-done.7, bf16[96,2048]{1,0:T(8,128)(2,1)} %collective-permute-done.6, bf16[96,2048]{1,0:T(8,128)(2,1)} %multiply_convert_fusion.1), kind=kOutput, calls=%fused_computation.76 | convolution fusion | flops 2219311104 | bytes 9502720 | tf_op jit(solution)/shard_map/dot_general | solution.py:302
  322.9 5.1 %multiply_convert_fusion = bf16[384,1408]{1,0:T(8,128)(2,1)} fusion(f32[384,1408]{1,0:T(8,128)S(1)} %fusion.48, bf16[4096,1408]{1,0:T(8,128)(2,1)S(1)} %copy-done.17, s32[]{:T(128)S(6)} %select_n.205, bf16[192,2048]{1,0:T(8,128)(2,1)} %collective-permute-done.7, bf16[96,2048]{1,0:T(8,128)(2,1)} %collective-permute-done.6, ...), kind=kOutput, calls=%fused_computation.48 | convolution fusion | flops 2222555136 | bytes 10584068 | tf_op jit(solution)/shard_map/dot_general | solution.py:303
  328.0 4.3 %convolution_convert_fusion = bf16[192,2048]{1,0:T(8,128)(2,1)S(1)} fusion(bf16[1408,2048]{1,0:T(8,128)(2,1)} %all-gather.5.cloned.1.call-done, bf16[384,1408]{1,0:T(8,128)(2,1)} %multiply_convert_fusion), kind=kOutput, calls=%fused_computation.46 | convolution fusion | flops 1107689472 | bytes 7094272 | tf_op jit(solution)/shard_map/dot_general | solution.py:71
  332.5 2.3 collective-permute-done.15
  334.7 1.4 convert_add_fusion
  336.2 1.9 collective-permute-start.16
  338.1 9.4 %collective-permute-done.16 = bf16[96,2048]{1,0:T(8,128)(2,1)S(1)} collective-permute-done((bf16[96,2048]{1,0:T(8,128)(2,1)S(1)}, bf16[96,2048]{1,0:T(8,128)(2,1)S(1)}, u32[]{:S(2)}, u32[]{:S(2)}) %collective-permute-start.16) | collective-permute-done | bytes 393248 | tf_op jit(solution)/shard_map/ppermute | solution.py:46
  (186 shorter events, 64.1 us)
Async XLA Ops:
  6.5 180.3 %copy-start = (bf16[256,2048]{1,0:T(8,128)(2,1)S(1)}, bf16[256,2048]{1,0:T(8,128)(2,1)}, u32[]{:S(2)}) copy-start(bf16[256,2048]{1,0:T(8,128)(2,1)} %param.27) | copy-start | bytes 3145732
  6.5 310.0 %all-gather.3.cloned.1.call-start = ((), (), s32[]{:S(2)}) async-start(), calls=%async_computation | async-start | bytes 6488064 | tf_op jit(solution)/shard_map/all_gather | solution.py:262
  7.3 320.8 %all-gather.5.cloned.1.call-start = ((), (), s32[]{:S(2)}) async-start(), calls=%async_computation.1 | async-start | bytes 6488064 | tf_op jit(solution)/shard_map/all_gather | solution.py:269
  13.5 5.5 %copy-start.13 = (bf16[384,256]{1,0:T(8,128)(2,1)S(1)}, bf16[384,256]{1,0:T(8,128)(2,1)}, u32[]{:S(2)}) copy-start(bf16[384,256]{1,0:T(8,128)(2,1)} %param.18) | copy-start | bytes 589828
  14.1 5.3 %copy-start.15 = (bf16[384,256]{1,0:T(8,128)(2,1)S(1)}, bf16[384,256]{1,0:T(8,128)(2,1)}, u32[]{:S(2)}) copy-start(bf16[384,256]{1,0:T(8,128)(2,1)} %param.20) | copy-start | bytes 589828
  24.0 66.5 %copy-start.2 = (bf16[256,1408]{1,0:T(8,128)(2,1)S(1)}, bf16[256,1408]{1,0:T(8,128)(2,1)}, u32[]{:S(2)}) copy-start(bf16[256,1408]{1,0:T(8,128)(2,1)} %param.30) | copy-start | bytes 2162692
  75.8 72.4 %copy-start.19 = (f32[128]{0:T(128)S(1)}, f32[128]{0:T(128)}, u32[]{:S(2)}) copy-start(f32[128]{0:T(128)} %param.26) | copy-start | bytes 1540
  75.9 10.2 %collective-permute-start = (bf16[2,128,256]{2,1,0:T(8,128)(2,1)S(1)}, bf16[2,128,256]{2,1,0:T(8,128)(2,1)S(1)}, u32[]{:S(2)}, u32[]{:S(2)}) collective-permute-start(bf16[2,128,256]{2,1,0:T(8,128)(2,1)S(1)} %pad_maximum_fusion.6), channel_id=1, source_target_pairs={{0,4},{4,8},{8,12},{12,16},{16,20},{20,24},{24,28},{1,5},{5,9},{9,... | collective-permute-start | bytes 393224 | tf_op jit(solution)/shard_map/ppermute | solution.py:15
  86.1 45.7 %copy-start.14 = (bf16[2,128,256]{2,1,0:T(8,128)(2,1)}, bf16[2,128,256]{2,1,0:T(8,128)(2,1)S(1)}, u32[]{:S(2)}) copy-start(bf16[2,128,256]{2,1,0:T(8,128)(2,1)S(1)} %collective-permute-done) | copy-start | bytes 393220
  86.1 7.6 %collective-permute-start.1 = (bf16[2,128,256]{2,1,0:T(8,128)(2,1)S(1)}, bf16[2,128,256]{2,1,0:T(8,128)(2,1)S(1)}, u32[]{:S(2)}, u32[]{:S(2)}) collective-permute-start(bf16[2,128,256]{2,1,0:T(8,128)(2,1)S(1)} %collective-permute-done), channel_id=1, source_target_pairs={{0,4},{4,8},{8,12},{12,16},{16,20},{20,24},{24,28},{1,5},{5,9},{9,... | collective-permute-start | bytes 393224 | tf_op jit(solution)/shard_map/ppermute | solution.py:15
  90.5 31.8 %collective-permute-start.8 = (bf16[256,1408]{1,0:T(8,128)(2,1)S(1)}, bf16[256,1408]{1,0:T(8,128)(2,1)S(1)}, u32[]{:S(2)}, u32[]{:S(2)}) collective-permute-start(bf16[256,1408]{1,0:T(8,128)(2,1)S(1)} %copy-done.2), channel_id=1, source_target_pairs={{0,4},{4,8},{8,12},{12,16},{16,20},{20,24},{24,28},{28,0},{1,5},{5... | collective-permute-start | bytes 2162696 | tf_op jit(solution)/shard_map/ppermute | solution.py:265
  93.9 12.6 %collective-permute-start.2 = (bf16[2,128,256]{2,1,0:T(8,128)(2,1)S(1)}, bf16[2,128,256]{2,1,0:T(8,128)(2,1)S(1)}, u32[]{:S(2)}, u32[]{:S(2)}) collective-permute-start(bf16[2,128,256]{2,1,0:T(8,128)(2,1)S(1)} %pad_maximum_fusion.7), channel_id=1, source_target_pairs={{0,8},{4,12},{8,16},{12,20},{16,24},{20,28},{1,9},{5,13},{9,17},{1... | collective-permute-start | bytes 393224 | tf_op jit(solution)/shard_map/ppermute | solution.py:15
  106.8 25.0 %copy-start.12 = (f32[2,128,256]{2,1,0:T(8,128)}, f32[2,128,256]{2,1,0:T(8,128)S(1)}, u32[]{:S(2)}) copy-start(f32[2,128,256]{2,1,0:T(8,128)S(1)} %fusion.96) | copy-start | bytes 786436
  122.3 100.0 %copy-start.4 = (bf16[256,1408]{1,0:T(8,128)(2,1)}, bf16[256,1408]{1,0:T(8,128)(2,1)S(1)}, u32[]{:S(2)}) copy-start(bf16[256,1408]{1,0:T(8,128)(2,1)S(1)} %collective-permute-done.8) | copy-start | bytes 2162692
  122.3 24.9 %collective-permute-start.9 = (bf16[256,1408]{1,0:T(8,128)(2,1)S(1)}, bf16[256,1408]{1,0:T(8,128)(2,1)S(1)}, u32[]{:S(2)}, u32[]{:S(2)}) collective-permute-start(bf16[256,1408]{1,0:T(8,128)(2,1)S(1)} %collective-permute-done.8), channel_id=1, source_target_pairs={{0,4},{4,8},{8,12},{12,16},{16,20},{20,24},{24,28},{28,0},{1,5},{5... | collective-permute-start | bytes 2162696 | tf_op jit(solution)/shard_map/ppermute | solution.py:265
  125.8 7.5 %collective-permute-start.3 = (bf16[2,128,128]{2,1,0:T(8,128)(2,1)}, bf16[2,128,128]{2,1,0:T(8,128)(2,1)}, u32[]{:S(2)}, u32[]{:S(2)}) collective-permute-start(bf16[2,128,128]{2,1,0:T(8,128)(2,1)} %fusion.132), channel_id=1, source_target_pairs={{0,16},{4,20},{8,24},{12,28},{1,17},{5,21},{9,25},{13,29},{2,18},{... | collective-permute-start | bytes 196616 | tf_op jit(solution)/shard_map/ppermute | solution.py:15
  131.8 125.8 %copy-start.1 = (bf16[96,2048]{1,0:T(8,128)(2,1)S(1)}, bf16[96,2048]{1,0:T(8,128)(2,1)}, u32[]{:S(2)}) copy-start(bf16[96,2048]{1,0:T(8,128)(2,1)} %param.17) | copy-start | bytes 1179652
  134.5 149.6 %copy-start.18 = (f32[2048]{0:T(1024)S(1)}, f32[2048]{0:T(1024)}, u32[]{:S(2)}) copy-start(f32[2048]{0:T(1024)} %param.28) | copy-start | bytes 24580
  147.1 75.1 %copy-start.6 = (bf16[256,1408]{1,0:T(8,128)(2,1)}, bf16[256,1408]{1,0:T(8,128)(2,1)S(1)}, u32[]{:S(2)}) copy-start(bf16[256,1408]{1,0:T(8,128)(2,1)S(1)} %collective-permute-done.9) | copy-start | bytes 2162692
  147.1 39.7 %collective-permute-start.10 = (bf16[256,1408]{1,0:T(8,128)(2,1)S(1)}, bf16[256,1408]{1,0:T(8,128)(2,1)}, u32[]{:S(2)}, u32[]{:S(2)}) collective-permute-start(bf16[256,1408]{1,0:T(8,128)(2,1)S(1)} %collective-permute-done.9), channel_id=1, source_target_pairs={{0,4},{4,8},{8,12},{12,16},{16,20},{20,24},{24,28},{28,0},{1,5},{5... | collective-permute-start | bytes 2162696 | tf_op jit(solution)/shard_map/ppermute | solution.py:265
  186.8 35.4 %collective-permute-start.11 = (bf16[256,1408]{1,0:T(8,128)(2,1)}, bf16[256,1408]{1,0:T(8,128)(2,1)S(1)}, u32[]{:S(2)}, u32[]{:S(2)}) collective-permute-start(bf16[256,1408]{1,0:T(8,128)(2,1)} %collective-permute-done.10), channel_id=1, source_target_pairs={{0,4},{4,8},{8,12},{12,16},{16,20},{20,24},{24,28},{28,0},{1,5},{5... | collective-permute-start | bytes 2162696 | tf_op jit(solution)/shard_map/ppermute | solution.py:265
  187.2 35.0 %collective-permute-start.4 = (bf16[192,2048]{1,0:T(8,128)(2,1)S(1)}, bf16[192,2048]{1,0:T(8,128)(2,1)S(1)}, u32[]{:S(2)}, u32[]{:S(2)}) collective-permute-start(bf16[192,2048]{1,0:T(8,128)(2,1)S(1)} %convolution_convert_fusion.1), channel_id=1, source_target_pairs={{0,1},{1,0},{2,3},{3,2},{4,5},{5,4},{6,7},{7,6},{8,9},{9,8},{10,11... | collective-permute-start | bytes 2359304 | tf_op jit(solution)/shard_map/ppermute | solution.py:46
  222.2 35.4 %copy-start.8 = (bf16[256,1408]{1,0:T(8,128)(2,1)}, bf16[256,1408]{1,0:T(8,128)(2,1)S(1)}, u32[]{:S(2)}) copy-start(bf16[256,1408]{1,0:T(8,128)(2,1)S(1)} %collective-permute-done.11) | copy-start | bytes 2162692
  222.2 35.4 %collective-permute-start.12 = (bf16[256,1408]{1,0:T(8,128)(2,1)S(1)}, bf16[256,1408]{1,0:T(8,128)(2,1)S(1)}, u32[]{:S(2)}, u32[]{:S(2)}) collective-permute-start(bf16[256,1408]{1,0:T(8,128)(2,1)S(1)} %collective-permute-done.11), channel_id=1, source_target_pairs={{0,4},{4,8},{8,12},{12,16},{16,20},{20,24},{24,28},{28,0},{1,5},{5... | collective-permute-start | bytes 2162696 | tf_op jit(solution)/shard_map/ppermute | solution.py:265
  222.7 34.9 %collective-permute-start.5 = (bf16[96,2048]{1,0:T(8,128)(2,1)S(1)}, bf16[96,2048]{1,0:T(8,128)(2,1)S(1)}, u32[]{:S(2)}, u32[]{:S(2)}) collective-permute-start(bf16[96,2048]{1,0:T(8,128)(2,1)S(1)} %slice.148), channel_id=1, source_target_pairs={{0,2},{1,3},{2,0},{3,1},{4,6},{5,7},{6,4},{7,5},{8,10},{9,11},{10,... | collective-permute-start | bytes 1179656 | tf_op jit(solution)/shard_map/ppermute | solution.py:46
  257.6 0.9 copy-start.10
  257.6 26.5 %collective-permute-start.13 = (bf16[256,1408]{1,0:T(8,128)(2,1)S(1)}, bf16[256,1408]{1,0:T(8,128)(2,1)}, u32[]{:S(2)}, u32[]{:S(2)}) collective-permute-start(bf16[256,1408]{1,0:T(8,128)(2,1)S(1)} %collective-permute-done.12), channel_id=1, source_target_pairs={{0,4},{4,8},{8,12},{12,16},{16,20},{20,24},{24,28},{28,0},{1,5},{5... | collective-permute-start | bytes 2162696 | tf_op jit(solution)/shard_map/ppermute | solution.py:265
  284.1 18.8 %collective-permute-start.14 = (bf16[256,1408]{1,0:T(8,128)(2,1)}, bf16[256,1408]{1,0:T(8,128)(2,1)}, u32[]{:S(2)}, u32[]{:S(2)}) collective-permute-start(bf16[256,1408]{1,0:T(8,128)(2,1)} %collective-permute-done.13), channel_id=1, source_target_pairs={{0,4},{4,8},{8,12},{12,16},{16,20},{20,24},{24,28},{28,0},{1,5},{5... | collective-permute-start | bytes 2162696 | tf_op jit(solution)/shard_map/ppermute | solution.py:265
  285.1 9.2 %collective-permute-start.6 = (bf16[96,2048]{1,0:T(8,128)(2,1)}, bf16[96,2048]{1,0:T(8,128)(2,1)}, u32[]{:S(2)}, u32[]{:S(2)}) collective-permute-start(bf16[96,2048]{1,0:T(8,128)(2,1)} %multiply_convert_fusion.1), channel_id=1, source_target_pairs={{0,2},{1,3},{2,0},{3,1},{4,6},{5,7},{6,4},{7,5},{8,10},{9,11},{10,... | collective-permute-start | bytes 1179656 | tf_op jit(solution)/shard_map/ppermute | solution.py:46
  286.7 19.8 %copy-start.9 = (bf16[256,1408]{1,0:T(8,128)(2,1)S(1)}, bf16[256,1408]{1,0:T(8,128)(2,1)}, u32[]{:S(2)}) copy-start(bf16[256,1408]{1,0:T(8,128)(2,1)} %copy-done.8) | copy-start | bytes 2162692
  286.7 21.1 %copy-start.7 = (bf16[256,1408]{1,0:T(8,128)(2,1)S(1)}, bf16[256,1408]{1,0:T(8,128)(2,1)}, u32[]{:S(2)}) copy-start(bf16[256,1408]{1,0:T(8,128)(2,1)} %copy-done.6) | copy-start | bytes 2162692
  286.7 21.2 %copy-start.5 = (bf16[256,1408]{1,0:T(8,128)(2,1)S(1)}, bf16[256,1408]{1,0:T(8,128)(2,1)}, u32[]{:S(2)}) copy-start(bf16[256,1408]{1,0:T(8,128)(2,1)} %copy-done.4) | copy-start | bytes 2162692
  286.7 21.3 %copy-start.3 = (bf16[256,1408]{1,0:T(8,128)(2,1)S(1)}, bf16[256,1408]{1,0:T(8,128)(2,1)}, u32[]{:S(2)}) copy-start(bf16[256,1408]{1,0:T(8,128)(2,1)} %param.30) | copy-start | bytes 2162692
  295.4 21.1 %collective-permute-start.7 = (bf16[192,2048]{1,0:T(8,128)(2,1)S(1)}, bf16[192,2048]{1,0:T(8,128)(2,1)}, u32[]{:S(2)}, u32[]{:S(2)}) collective-permute-start(bf16[192,2048]{1,0:T(8,128)(2,1)S(1)} %pad_maximum_fusion.1), channel_id=1, source_target_pairs={{0,1},{1,0},{2,3},{3,2},{4,5},{5,4},{6,7},{7,6},{8,9},{9,8},{10,11... | collective-permute-start | bytes 2359304 | tf_op jit(solution)/shard_map/ppermute | solution.py:46
  305.2 5.3 %copy-start.11 = (bf16[256,1408]{1,0:T(8,128)(2,1)S(1)}, bf16[256,1408]{1,0:T(8,128)(2,1)}, u32[]{:S(2)}) copy-start(bf16[256,1408]{1,0:T(8,128)(2,1)} %copy-done.10) | copy-start | bytes 2162692
  312.2 4.3 %copy-start.16 = (bf16[4096,1408]{1,0:T(8,128)(2,1)}, bf16[4096,1408]{1,0:T(8,128)(2,1)S(1)}, u32[]{:S(2)}) copy-start(bf16[4096,1408]{1,0:T(8,128)(2,1)S(1)} %constant_dynamic-update-slice_fusion) | copy-start | bytes 34603012
  316.5 6.4 %copy-start.17 = (bf16[4096,1408]{1,0:T(8,128)(2,1)S(1)}, bf16[4096,1408]{1,0:T(8,128)(2,1)}, u32[]{:S(2)}) copy-start(bf16[4096,1408]{1,0:T(8,128)(2,1)} %copy-done.16) | copy-start | bytes 34603012
  328.0 6.7 %copy-start.20 = (bf16[1408,2048]{1,0:T(8,128)(2,1)S(1)}, bf16[1408,2048]{1,0:T(8,128)(2,1)}, u32[]{:S(2)}) copy-start(bf16[1408,2048]{1,0:T(8,128)(2,1)} %all-gather.5.cloned.1.call-done) | copy-start | bytes 17301508
  328.0 6.7 %copy-start.21 = (bf16[384,1408]{1,0:T(8,128)(2,1)S(1)}, bf16[384,1408]{1,0:T(8,128)(2,1)}, u32[]{:S(2)}) copy-start(bf16[384,1408]{1,0:T(8,128)(2,1)} %multiply_convert_fusion) | copy-start | bytes 3244036
  332.4 2.4 collective-permute-start.15
  336.2 11.4 %collective-permute-start.16 = (bf16[96,2048]{1,0:T(8,128)(2,1)S(1)}, bf16[96,2048]{1,0:T(8,128)(2,1)S(1)}, u32[]{:S(2)}, u32[]{:S(2)}) collective-permute-start(bf16[96,2048]{1,0:T(8,128)(2,1)S(1)} %slice.147), channel_id=1, source_target_pairs={{0,2},{1,3},{2,0},{3,1},{4,6},{5,7},{6,4},{7,5},{8,10},{9,11},{10,... | collective-permute-start | bytes 1179656 | tf_op jit(solution)/shard_map/ppermute | solution.py:46
Sparse Core Ops, SparseCore 0:
  9.5 96.1 all-gather.2
  131.9 132.9 all-gather.4
